TPU v7x, 256 devices: a whole 4x4x8 slice. The times are simulated.
256 devices in a mesh: sp: 64 (over z, x, core), tp: 4 (over y).
Axes of the slice: x: 4, y: 4, z: 8, core: 2. Of those that a mesh axis runs over, the one named last changes fastest.
Arguments:
- residual_in: bfloat16 [16384, 2048], P('sp', 'tp'), may hold values from -6 to 6
- conv_input: bfloat16 [16384, 512], P('sp', 'tp'), may hold values from -6 to 6
- outer_gate: bfloat16 [16384, 512], P('sp', 'tp'), may hold values from -6 to 6
- inner_gate: bfloat16 [16384, 512], P('sp', 'tp'), may hold values from -6 to 6
- documents: int32 [16384], P('sp'), may hold values from 0 to 31, as said below
- conv_taps: float32 [3, 512], P(None, 'tp'), may hold values from -3 to 3
- mixer_gain: float32 [512], replicated, may hold values from 0.1 to 1.9
- output_weight: bfloat16 [512, 2048], P(None, 'tp'), may hold values from -0.25 to 0.25
- ffn_gain: float32 [2048], P('tp'), may hold values from 0.1 to 1.9
- routes: int32 [16384, 2], P('sp'), may hold values from 0 to 63, all different within a row; in each aligned block of 256 rows (0 to 255, 256 to 511, ...) at most 16 rows name the same one
- route_weights: float32 [16384, 2], P('sp'), may hold values from 0.1 to 0.9
- expert_gate: bfloat16 [64, 2048, 3584], P('sp', None, 'tp'), may hold values from -0.125 to 0.125
- expert_up: bfloat16 [64, 2048, 3584], P('sp', None, 'tp'), may hold values from -0.125 to 0.125
- expert_down: bfloat16 [64, 3584, 2048], P('sp', 'tp'), may hold values from -0.09375 to 0.09375
Outputs:
- layer_out: bfloat16 [16384, 2048], P('sp', 'tp')
Inputs may be any that keep to these rules, and one draw needn't show every extreme that they name: Document numbers never fall along the positions, and each of the 32 documents occurs. Every document has 256 to 768 positions, and one has exactly 768. `routes`: the two experts of a position differ. Among the 256 positions of one index of sp no expert is named more than 16 times, a bound that some block reaches.
All inputs are finite; a program needn't handle non-finite values.
Results may differ from a plain program's by a relative error of at most 0.0058.
Values may be sent and summed in bfloat16 or wider, within the bound.
A program may use at most 64 MiB of HBM per device.

v0:
```python
import jax
import jax.numpy as jnp
from jax import lax
from jax.sharding import PartitionSpec as P

EPS = 1e-06


def from_behind(block, axis, distance):
    devices = range(lax.axis_size(axis))
    route = [(i - distance, i) for i in devices if i - distance in devices]
    return lax.ppermute(block, axis, route)


def laid_out(pieces, dim):
    dims = list(pieces.shape[1:])
    dims[dim] *= pieces.shape[0]
    return jnp.moveaxis(pieces, 0, dim).reshape(dims)


def sent_to_all(shard, axis):
    copies = jnp.broadcast_to(shard, (lax.axis_size(axis), *shard.shape))
    return lax.all_to_all(copies, axis, split_axis=0, concat_axis=0, tiled=True)


def gather_directly(shard, axis, dim):
    return laid_out(sent_to_all(shard, axis), dim)


def over_copies(shard, axis):
    return sent_to_all(shard, axis).sum(axis=0)


def slot_tables(routes, experts, capacity):
    tokens = routes.shape[0]
    flattened = routes.reshape(-1)
    onehot = (flattened[:, None] == jnp.arange(experts, dtype=jnp.int32)[None, :]).astype(jnp.int32)
    earlier = jnp.cumsum(onehot, axis=0) - onehot
    position_in = jnp.sum(earlier * onehot, axis=1)
    target = flattened * capacity + position_in
    owners = (
        jnp.full((experts * capacity,), tokens, jnp.int32)
        .at[target]
        .set(jnp.arange(2 * tokens, dtype=jnp.int32) // 2)
    )
    return (target, owners)


def per_device(
    residual_in,
    conv_input,
    outer_gate,
    inner_gate,
    documents,
    conv_taps,
    mixer_gain,
    output_weight,
    ffn_gain,
    routes,
    route_weights,
    expert_gate,
    expert_up,
    expert_down,
):
    tokens_here = residual_in.shape[0]
    local_features = residual_in.shape[1]
    conv_value = (inner_gate.astype(jnp.float32) * conv_input.astype(jnp.float32)).astype(
        jnp.bfloat16
    )
    doc_marks = documents.astype(jnp.bfloat16)
    before_rows, before_docs = from_behind((conv_value[-2:], doc_marks[-2:]), "sp", 1)
    joined_rows = jnp.concatenate([before_rows, conv_value], axis=0).astype(jnp.float32)
    joined_docs = jnp.concatenate([before_docs, doc_marks], axis=0)
    same_one = (joined_docs[1:-1] == doc_marks).astype(jnp.float32)[:, None]
    same_two = (joined_docs[:-2] == doc_marks).astype(jnp.float32)[:, None]
    conv_sum = (
        conv_taps[2] * joined_rows[2:]
        + conv_taps[1] * joined_rows[1:-1] * same_one
        + conv_taps[0] * joined_rows[:-2] * same_two
    )
    mixed = (outer_gate.astype(jnp.float32) * conv_sum).astype(jnp.bfloat16)
    piece_f = gather_directly(mixed, "tp", 1).astype(jnp.float32)
    scaled = (piece_f * mixer_gain).astype(jnp.bfloat16)
    accum = jnp.dot(scaled, output_weight, preferred_element_type=jnp.float32)
    squares = jnp.sum(piece_f * piece_f, axis=1)
    mix_scale = lax.rsqrt(squares / mixer_gain.shape[0] + EPS)
    hidden_state = residual_in.astype(jnp.float32) + accum * mix_scale[:, None]
    feature_total = over_copies(jnp.sum(hidden_state * hidden_state, axis=1), "tp")
    model_width = local_features * lax.axis_size("tp")
    normed = (
        hidden_state * lax.rsqrt(feature_total / model_width + EPS)[:, None] * ffn_gain
    ).astype(jnp.bfloat16)
    experts = lax.axis_size("sp") * expert_gate.shape[0]
    capacity = 4 * tokens_here // experts
    target, owners = slot_tables(routes, experts, capacity)
    padded = jnp.concatenate([normed, jnp.zeros((1, local_features), jnp.bfloat16)], axis=0)
    outgoing = padded[owners].reshape(experts, capacity, local_features)
    slices_in = lax.all_to_all(outgoing, "sp", split_axis=0, concat_axis=0, tiled=True)
    arrived = lax.all_gather(slices_in, "tp", axis=2, tiled=True)
    expert_in = arrived.reshape(-1, model_width)
    gate = jnp.dot(expert_in, expert_gate[0], preferred_element_type=jnp.float32)
    upper = jnp.dot(expert_in, expert_up[0], preferred_element_type=jnp.float32)
    act = (jax.nn.silu(gate) * upper).astype(jnp.bfloat16)
    partial_out = jnp.dot(act, expert_down[0], preferred_element_type=jnp.float32)
    summed = lax.psum_scatter(
        partial_out.astype(jnp.bfloat16), "tp", scatter_dimension=1, tiled=True
    )
    returned = lax.all_to_all(
        summed.reshape(experts, capacity, local_features),
        "sp",
        split_axis=0,
        concat_axis=0,
        tiled=True,
    )
    picked = returned.reshape(experts * capacity, local_features)[target].astype(jnp.float32)
    picked = picked.reshape(tokens_here, 2, local_features)
    routed = jnp.sum(picked * route_weights[:, :, None], axis=1)
    return (hidden_state + routed).astype(jnp.bfloat16)


def solution(mesh):
    placed = (
        P("sp", "tp"),
        P("sp", "tp"),
        P("sp", "tp"),
        P("sp", "tp"),
        P("sp"),
        P(None, "tp"),
        P(),
        P(None, "tp"),
        P("tp"),
        P("sp", None),
        P("sp", None),
        P("sp", None, "tp"),
        P("sp", None, "tp"),
        P("sp", "tp", None),
    )
    return jax.shard_map(
        per_device, mesh=mesh, in_specs=placed, out_specs=P("sp", "tp"), check_vma=False
    )
```

profile of v0, /device:TPU:1, one launch (start us, length us, event | category | flops | bytes accessed | tf_op | source)
XLA Modules:
  0.0 252.4 jit_solution(10328017283454354348)
XLA Ops:
  6.5 0.8 convert_element_type.78
  7.4 4.5 %collective-permute-start.1 = (bf16[2]{0:T(256)(128)(2,1)S(1)}, bf16[2]{0:T(256)(128)(2,1)S(1)}, u32[]{:S(2)}, u32[]{:S(2)}) collective-permute-start(bf16[2]{0:T(256)(128)(2,1)S(1)} %slice.41), channel_id=1, source_target_pairs={{0,4},{4,8},{8,12},{12,16},{16,20},{20,24},{24,28},{28,32},{32,36}... | collective-permute-start | bytes 20 | tf_op jit(solution)/shard_map/ppermute | solution.py:12
  11.9 0.9 multiply_convert_fusion.2
  12.8 1.9 collective-permute-start
  14.7 0.8 copy.31
  15.8 0.7 broadcast_multiply_fusion
  16.5 0.8 slice_bitcast_fusion.2
  17.3 1.2 reduce-window.6
  19.3 0.8 compare_convert_fusion.1
  20.1 1.0 fusion.15
  21.2 0.7 broadcast_in_dim.8
  21.9 4.2 %all-to-all-start = ((bf16[4,256,128]{1,2,0:T(8,128)(2,1)}), bf16[4,256,128]{1,2,0:T(8,128)(2,1)S(1)}, u32[]{:S(2)}, u32[]{:S(2)}) async-start(bf16[4,256,128]{1,2,0:T(8,128)(2,1)} %broadcast_in_dim.8), calls=%async_computation | async-start | bytes 524288 | tf_op jit(solution)/shard_map/all_to_all | solution.py:23
  26.1 2.4 scatter_custom_fusion
  28.5 3.2 %all-to-all-done = bf16[4,256,128]{1,2,0:T(8,128)(2,1)S(1)} async-done(((bf16[4,256,128]{1,2,0:T(8,128)(2,1)}), bf16[4,256,128]{1,2,0:T(8,128)(2,1)S(1)}, u32[]{:S(2)}, u32[]{:S(2)}) %all-to-all-start) | async-done | bytes 262176 | tf_op jit(solution)/shard_map/all_to_all | solution.py:23
  31.9 0.8 fusion.8
  32.7 0.4 multiply_reduce_fusion.1
  33.2 0.6 broadcast_in_dim.9
  33.8 3.2 %all-to-all-start.1 = ((f32[4,1,256]{2,1,0:T(1,128)}), f32[4,1,256]{2,1,0:T(1,128)S(1)}, u32[]{:S(2)}, u32[]{:S(2)}) async-start(f32[4,1,256]{2,1,0:T(1,128)} %broadcast_in_dim.9), calls=%async_computation.1 | async-start | bytes 8192 | tf_op jit(solution)/shard_map/all_to_all | solution.py:23
  37.1 4.0 %all-to-all-done.1 = f32[4,1,256]{2,1,0:T(1,128)S(1)} async-done(((f32[4,1,256]{2,1,0:T(1,128)}), f32[4,1,256]{2,1,0:T(1,128)S(1)}, u32[]{:S(2)}, u32[]{:S(2)}) %all-to-all-start.1) | async-done | bytes 4128 | tf_op jit(solution)/shard_map/all_to_all | solution.py:23
  41.3 4.0 %gather_fusion = bf16[1024,512]{1,0:T(8,128)(2,1)S(1)} fusion(bf16[257,512]{1,0:T(8,128)(2,1)S(1)} %concatenate.11, s32[1024]{0:T(1024)S(1)} %fusion.19), kind=kCustom, calls=%fused_computation | custom fusion | bytes 2101248 | tf_op jit(solution)/shard_map/gather | solution.py:97
  45.3 42.3 %all_to_all.21 = bf16[64,16,512]{2,1,0:T(8,128)(2,1)} all-to-all(bf16[64,16,512]{2,1,0:T(8,128)(2,1)S(1)} %bitcast.54), channel_id=1, replica_groups=mesh['sp'=64,'tp'=4] {'sp'}, dimensions={0} | all-to-all | bytes 2097152 | tf_op jit(solution)/shard_map/all_to_all | solution.py:98
  87.7 45.8 %all-gather.2.cloned.1.call-done = bf16[64,16,2048]{2,1,0:T(8,128)(2,1)} async-done(((bf16[64,16,512]{2,1,0:T(8,128)(2,1)}), bf16[64,16,2048]{2,1,0:T(8,128)(2,1)}) %all-gather.2.cloned.1.call-update) | async-done | bytes 4194320 | tf_op jit(solution)/shard_map/all_gather | solution.py:99
  133.5 7.5 %fusion.1 = f32[1024,896]{1,0:T(8,128)S(1)} fusion(bf16[1024,2048]{1,0:T(8,128)(2,1)} %bitcast.59, bf16[1,2048,896]{2,1,0:T(8,128)(2,1)} %param.26), kind=kOutput, calls=%fused_computation.5 | convolution fusion | flops 3758096384 | bytes 11534336 | tf_op jit(solution)/shard_map/dot_general | solution.py:102
  141.0 4.8 %multiply_convert_fusion = bf16[1024,896]{1,0:T(8,128)(2,1)S(1)} fusion(f32[1024,896]{1,0:T(8,128)S(1)} %fusion.1, bf16[1024,2048]{1,0:T(8,128)(2,1)S(1)} %bitcast.60, bf16[1,2048,896]{2,1,0:T(8,128)(2,1)S(1)} %copy-done.5), kind=kOutput, calls=%fused_computation.9 | convolution fusion | flops 3763601408 | bytes 13369344 | tf_op jit(solution)/shard_map/dot_general | solution.py:101
  145.9 6.1 %convolution_convert_fusion = bf16[1024,2048]{1,0:T(8,128)(2,1)} fusion(bf16[1024,896]{1,0:T(8,128)(2,1)S(1)} %multiply_convert_fusion, bf16[1,896,2048]{2,1,0:T(8,128)(2,1)S(1)} %copy-done.6), kind=kOutput, calls=%fused_computation.3 | convolution fusion | flops 3760193536 | bytes 9699328 | tf_op jit(solution)/shard_map/dot_general | solution.py:104
  151.9 50.0 %reduce-scatter.2.cloned.1.call-done = bf16[1024,512]{1,0:T(8,128)(2,1)} async-done(((bf16[1024,2048]{1,0:T(8,128)(2,1)}), bf16[1024,512]{1,0:T(8,128)(2,1)}) %reduce-scatter.2.cloned.1.call-update) | async-done | bytes 1048592 | tf_op jit(solution)/shard_map/reduce_scatter | solution.py:105
  202.0 10.7 %all-to-all-start.3 = ((bf16[64,16,512]{2,1,0:T(8,128)(2,1)}), bf16[64,16,512]{2,1,0:T(8,128)(2,1)S(1)}, u32[]{:S(2)}, u32[]{:S(2)}) async-start(bf16[64,16,512]{2,1,0:T(8,128)(2,1)} %bitcast.55), calls=%async_computation.4 | async-start | bytes 2097152 | tf_op jit(solution)/shard_map/all_to_all | solution.py:108
  212.8 28.0 %all-to-all-done.3 = bf16[64,16,512]{2,1,0:T(8,128)(2,1)S(1)} async-done(((bf16[64,16,512]{2,1,0:T(8,128)(2,1)}), bf16[64,16,512]{2,1,0:T(8,128)(2,1)S(1)}, u32[]{:S(2)}, u32[]{:S(2)}) %all-to-all-start.3) | async-done | bytes 1048608 | tf_op jit(solution)/shard_map/all_to_all | solution.py:108
  240.8 2.0 gather_fusion.1
  242.8 0.7 reshape.90
  243.5 1.3 multiply_reduce_fusion
  244.8 0.8 add_convert_fusion
  (45 shorter events, 1.8 us)
Async XLA Ops:
  6.5 26.2 %copy-start = (bf16[512,512]{1,0:T(8,128)(2,1)S(1)}, bf16[512,512]{1,0:T(8,128)(2,1)}, u32[]{:S(2)}) copy-start(bf16[512,512]{1,0:T(8,128)(2,1)} %param.21) | copy-start | bytes 1572868
  6.5 26.2 %copy-start.1 = (bf16[256,512]{1,0:T(8,128)(2,1)S(1)}, bf16[256,512]{1,0:T(8,128)(2,1)}, u32[]{:S(2)}) copy-start(bf16[256,512]{1,0:T(8,128)(2,1)} %param.14) | copy-start | bytes 786436
  6.5 34.6 %copy-start.2 = (f32[512]{0:T(512)S(1)}, f32[512]{0:T(512)}, u32[]{:S(2)}) copy-start(f32[512]{0:T(512)} %param.22) | copy-start | bytes 6148
  7.4 11.8 %collective-permute-start.1 = (bf16[2]{0:T(256)(128)(2,1)S(1)}, bf16[2]{0:T(256)(128)(2,1)S(1)}, u32[]{:S(2)}, u32[]{:S(2)}) collective-permute-start(bf16[2]{0:T(256)(128)(2,1)S(1)} %slice.41), channel_id=1, source_target_pairs={{0,4},{4,8},{8,12},{12,16},{16,20},{20,24},{24,28},{28,32},{32,36}... | collective-permute-start | bytes 20 | tf_op jit(solution)/shard_map/ppermute | solution.py:12
  12.8 7.3 %collective-permute-start = (bf16[2,128]{1,0:T(2,128)(2,1)S(1)}, bf16[2,128]{1,0:T(2,128)(2,1)S(1)}, u32[]{:S(2)}, u32[]{:S(2)}) collective-permute-start(bf16[2,128]{1,0:T(2,128)(2,1)S(1)} %slice.52), channel_id=1, source_target_pairs={{0,4},{4,8},{8,12},{12,16},{16,20},{20,24},{24,28},{28,32},{32,36}... | collective-permute-start | bytes 1544 | tf_op jit(solution)/shard_map/ppermute | solution.py:12
  21.9 9.9 %all-to-all-start = ((bf16[4,256,128]{1,2,0:T(8,128)(2,1)}), bf16[4,256,128]{1,2,0:T(8,128)(2,1)S(1)}, u32[]{:S(2)}, u32[]{:S(2)}) async-start(bf16[4,256,128]{1,2,0:T(8,128)(2,1)} %broadcast_in_dim.8), calls=%async_computation | async-start | bytes 524288 | tf_op jit(solution)/shard_map/all_to_all | solution.py:23
  33.8 7.4 %all-to-all-start.1 = ((f32[4,1,256]{2,1,0:T(1,128)}), f32[4,1,256]{2,1,0:T(1,128)S(1)}, u32[]{:S(2)}, u32[]{:S(2)}) async-start(f32[4,1,256]{2,1,0:T(1,128)} %broadcast_in_dim.9), calls=%async_computation.1 | async-start | bytes 8192 | tf_op jit(solution)/shard_map/all_to_all | solution.py:23
  37.0 96.5 %all-gather.2.cloned.1.call-start = ((), (), s32[]{:S(2)}) async-start(), calls=%async_computation.5 | async-start | bytes 5242880 | tf_op jit(solution)/shard_map/all_gather | solution.py:99
  87.7 114.3 %reduce-scatter.2.cloned.1.call-start = ((), (), s32[]{:S(2)}) async-start(), calls=%async_computation.6 | async-start | bytes 5242880 | tf_op jit(solution)/shard_map/reduce_scatter | solution.py:105
  133.5 7.5 %copy-start.4 = (bf16[64,16,2048]{2,1,0:T(8,128)(2,1)S(1)}, bf16[64,16,2048]{2,1,0:T(8,128)(2,1)}, u32[]{:S(2)}) copy-start(bf16[64,16,2048]{2,1,0:T(8,128)(2,1)} %all-gather.2.cloned.1.call-done) | copy-start | bytes 12582916
  133.5 7.5 %copy-start.5 = (bf16[1,2048,896]{2,1,0:T(8,128)(2,1)S(1)}, bf16[1,2048,896]{2,1,0:T(8,128)(2,1)}, u32[]{:S(2)}) copy-start(bf16[1,2048,896]{2,1,0:T(8,128)(2,1)} %param.25) | copy-start | bytes 11010052
  141.0 4.8 %copy-start.6 = (bf16[1,896,2048]{2,1,0:T(8,128)(2,1)S(1)}, bf16[1,896,2048]{2,1,0:T(8,128)(2,1)}, u32[]{:S(2)}) copy-start(bf16[1,896,2048]{2,1,0:T(8,128)(2,1)} %param.27) | copy-start | bytes 11010052
  151.9 60.8 %copy-start.3 = (f32[256,2]{0,1:T(2,128)S(1)}, f32[256,2]{0,1:T(2,128)}, u32[]{:S(2)}) copy-start(f32[256,2]{0,1:T(2,128)} %param.24) | copy-start | bytes 6148
  202.0 38.9 %all-to-all-start.3 = ((bf16[64,16,512]{2,1,0:T(8,128)(2,1)}), bf16[64,16,512]{2,1,0:T(8,128)(2,1)S(1)}, u32[]{:S(2)}, u32[]{:S(2)}) async-start(bf16[64,16,512]{2,1,0:T(8,128)(2,1)} %bitcast.55), calls=%async_computation.4 | async-start | bytes 2097152 | tf_op jit(solution)/shard_map/all_to_all | solution.py:108
Sparse Core Ops, SparseCore 0:
  87.8 45.6 all-gather.1
  152.1 49.8 reduce-scatter.1
where the time goes:
time: 253 us; the launch traced here: 252 us
  waiting for transfers between devices  131 us (52%)
  blocking collectives  42.3 us (17%)
  starting transfers between devices  24.6 us (10%)
  matrix products  18.8 us (7%)
  between operations  13.7 us (5%)
  local copies, waits for them, and re-layouts  13.1 us (5%)
  other arithmetic  8.73 us (3%)
    reduce_scatter x1, waiting for transfers between devices, per_device(): lax.psum_scatter(partial_out.astype(jnp.bfloat16), 'tp', scatter_dimensio...  50 us
    all_gather x1, waiting for transfers between devices, per_device(): arrived = lax.all_gather(slices_in, 'tp', axis=2, tiled=True)  45.8 us
    all_to_all x1, blocking collectives, per_device(): lax.all_to_all(outgoing, 'sp', split_axis=0, concat_axis=0, tiled=True)  42.3 us
    all_to_all x1, waiting for transfers between devices, per_device(): lax.all_to_all(summed.reshape(experts, capacity, local_features), 'sp', s...  28 us
    all_to_all x1, starting transfers between devices, per_device(): lax.all_to_all(summed.reshape(experts, capacity, local_features), 'sp', s...  10.7 us
    dot_general x1, matrix products, per_device(): upper = jnp.dot(expert_in, expert_up[0], preferred_element_type=jnp.float32)  7.49 us
    all_to_all x2, starting transfers between devices, sent_to_all(): return lax.all_to_all(copies, axis, split_axis=0, concat_axis=0, tiled=True)  7.43 us
    all_to_all x2, waiting for transfers between devices, sent_to_all(): return lax.all_to_all(copies, axis, split_axis=0, concat_axis=0, tiled=True)  7.29 us
  transfers between devices with their start and end apart: 7, of which 5 were waited for; matrix products, arithmetic and copies ran while one was open for 3% of the time, Pallas kernels for 0%

commit v1 on v0

--- a/solution.py
+++ b/solution.py
@@ -96,7 +96,12 @@
     padded = jnp.concatenate([normed, jnp.zeros((1, local_features), jnp.bfloat16)], axis=0)
     outgoing = padded[owners].reshape(experts, capacity, local_features)
     slices_in = lax.all_to_all(outgoing, "sp", split_axis=0, concat_axis=0, tiled=True)
-    arrived = lax.all_gather(slices_in, "tp", axis=2, tiled=True)
+    ring = [slices_in]
+    for hop in range(3):
+        ring.append(lax.ppermute(ring[-1], "tp", [(dev, (dev + 1) % 4) for dev in range(4)]))
+    arrived = jnp.roll(
+        jnp.concatenate(ring[::-1], axis=2), (lax.axis_index("tp") + 1) * ring[0].shape[2], axis=2
+    )
     expert_in = arrived.reshape(-1, model_width)
     gate = jnp.dot(expert_in, expert_gate[0], preferred_element_type=jnp.float32)
     upper = jnp.dot(expert_in, expert_up[0], preferred_element_type=jnp.float32)

time: 253 us -> 284 us (1.12)
  waiting for transfers between devices: 131 us -> 156 us
  local copies, waits for them, and re-layouts: 13.1 us -> 21.3 us
    ppermute x0 -> x3, waiting for transfers between devices: none -> 71.9 us  [per_device(): lax.ppermute(ring[-1], 'tp', [(dev, (dev + 1) % 4) for dev in range(4)])]
    all_gather x1 -> x0, waiting for transfers between devices: 45.8 us -> none  [per_device(): arrived = lax.all_gather(slices_in, 'tp', axis=2, tiled=True)]
    unnamed x16 -> x21, local copies, waits for them, and re-layouts: 0.97 us -> 8.65 us
  transfers between devices with their start and end apart: 7 -> 9, of which waited for: 5 -> 7; matrix products, arithmetic and copies ran while one was open for 3% -> 3% of each run, Pallas kernels for 0% -> 0%
where the time goes in v1:
time: 284 us; the launch traced here: 283 us
  waiting for transfers between devices  156 us (55%)
  blocking collectives  42.2 us (15%)
  starting transfers between devices  24.9 us (9%)
  local copies, waits for them, and re-layouts  21.3 us (8%)
  matrix products  16.6 us (6%)
  between operations  13.7 us (5%)
  other arithmetic  8.71 us (3%)
    ppermute x3, waiting for transfers between devices, per_device(): lax.ppermute(ring[-1], 'tp', [(dev, (dev + 1) % 4) for dev in range(4)])  71.9 us
    reduce_scatter x1, waiting for transfers between devices, per_device(): lax.psum_scatter(partial_out.astype(jnp.bfloat16), 'tp', scatter_dimensio...  48.8 us
    all_to_all x1, blocking collectives, per_device(): lax.all_to_all(outgoing, 'sp', split_axis=0, concat_axis=0, tiled=True)  42.2 us
    all_to_all x1, waiting for transfers between devices, per_device(): lax.all_to_all(summed.reshape(experts, capacity, local_features), 'sp', s...  28 us
    all_to_all x1, starting transfers between devices, per_device(): lax.all_to_all(summed.reshape(experts, capacity, local_features), 'sp', s...  10.7 us
    unnamed x21, local copies, waits for them, and re-layouts  8.65 us
    all_to_all x2, starting transfers between devices, sent_to_all(): return lax.all_to_all(copies, axis, split_axis=0, concat_axis=0, tiled=True)  7.43 us
    all_to_all x2, waiting for transfers between devices, sent_to_all(): return lax.all_to_all(copies, axis, split_axis=0, concat_axis=0, tiled=True)  7.29 us
  transfers between devices with their start and end apart: 9, of which 7 were waited for; matrix products, arithmetic and copies ran while one was open for 3% of the time, Pallas kernels for 0%

profile of v1, /device:TPU:1, one launch (start us, length us, event | category | flops | bytes accessed | tf_op | source)
XLA Modules:
  0.0 283.4 jit_solution(13396922570356189599)
XLA Ops:
  7.4 4.5 %collective-permute-start.1 = (bf16[2]{0:T(256)(128)(2,1)S(1)}, bf16[2]{0:T(256)(128)(2,1)S(1)}, u32[]{:S(2)}, u32[]{:S(2)}) collective-permute-start(bf16[2]{0:T(256)(128)(2,1)S(1)} %slice.41), channel_id=1, source_target_pairs={{0,4},{4,8},{8,12},{12,16},{16,20},{20,24},{24,28},{28,32},{32,36}... | collective-permute-start | bytes 20 | tf_op jit(solution)/shard_map/ppermute | solution.py:12
  11.9 0.9 multiply_convert_fusion.2
  12.8 1.9 collective-permute-start
  14.7 0.8 copy.31
  16.5 0.8 slice_bitcast_fusion.2
  17.3 1.2 reduce-window.6
  20.1 1.0 fusion.15
  21.9 4.2 %all-to-all-start = ((bf16[4,256,128]{1,2,0:T(8,128)(2,1)}), bf16[4,256,128]{1,2,0:T(8,128)(2,1)S(1)}, u32[]{:S(2)}, u32[]{:S(2)}) async-start(bf16[4,256,128]{1,2,0:T(8,128)(2,1)} %broadcast_in_dim.8), calls=%async_computation | async-start | bytes 524288 | tf_op jit(solution)/shard_map/all_to_all | solution.py:23
  26.1 2.4 scatter_custom_fusion
  28.5 3.2 %all-to-all-done = bf16[4,256,128]{1,2,0:T(8,128)(2,1)S(1)} async-done(((bf16[4,256,128]{1,2,0:T(8,128)(2,1)}), bf16[4,256,128]{1,2,0:T(8,128)(2,1)S(1)}, u32[]{:S(2)}, u32[]{:S(2)}) %all-to-all-start) | async-done | bytes 262176 | tf_op jit(solution)/shard_map/all_to_all | solution.py:23
  31.9 0.8 fusion.8
  32.7 1.4 multiply_reduce_fusion.1
  34.7 3.2 %all-to-all-start.1 = ((f32[4,1,256]{2,1,0:T(1,128)}), f32[4,1,256]{2,1,0:T(1,128)S(1)}, u32[]{:S(2)}, u32[]{:S(2)}) async-start(f32[4,1,256]{2,1,0:T(1,128)} %broadcast_in_dim.9), calls=%async_computation.1 | async-start | bytes 8192 | tf_op jit(solution)/shard_map/all_to_all | solution.py:23
  38.0 4.0 %all-to-all-done.1 = f32[4,1,256]{2,1,0:T(1,128)S(1)} async-done(((f32[4,1,256]{2,1,0:T(1,128)}), f32[4,1,256]{2,1,0:T(1,128)S(1)}, u32[]{:S(2)}, u32[]{:S(2)}) %all-to-all-start.1) | async-done | bytes 4128 | tf_op jit(solution)/shard_map/all_to_all | solution.py:23
  42.2 4.0 %gather_fusion = bf16[1024,512]{1,0:T(8,128)(2,1)S(1)} fusion(bf16[257,512]{1,0:T(8,128)(2,1)S(1)} %concatenate.17, s32[1024]{0:T(1024)S(1)} %fusion.19), kind=kCustom, calls=%fused_computation | custom fusion | bytes 2101248 | tf_op jit(solution)/shard_map/gather | solution.py:97
  46.2 42.2 %all_to_all.21 = bf16[64,16,512]{2,1,0:T(8,128)(2,1)S(1)} all-to-all(bf16[64,16,512]{2,1,0:T(8,128)(2,1)S(1)} %bitcast.54), channel_id=1, replica_groups=mesh['sp'=64,'tp'=4] {'sp'}, dimensions={0} | all-to-all | bytes 2097152 | tf_op jit(solution)/shard_map/all_to_all | solution.py:98
  88.7 24.5 %collective-permute-done.2 = bf16[64,16,512]{2,1,0:T(8,128)(2,1)S(1)} collective-permute-done((bf16[64,16,512]{2,1,0:T(8,128)(2,1)S(1)}, bf16[64,16,512]{2,1,0:T(8,128)(2,1)S(1)}, u32[]{:S(2)}, u32[]{:S(2)}) %collective-permute-start.2) | collective-permute-done | bytes 1048608 | tf_op jit(solution)/shard_map/ppermute | solution.py:101
  113.2 24.0 %collective-permute-done.3 = bf16[64,16,512]{2,1,0:T(8,128)(2,1)} collective-permute-done((bf16[64,16,512]{2,1,0:T(8,128)(2,1)S(1)}, bf16[64,16,512]{2,1,0:T(8,128)(2,1)}, u32[]{:S(2)}, u32[]{:S(2)}) %collective-permute-start.3) | collective-permute-done | bytes 1048608 | tf_op jit(solution)/shard_map/ppermute | solution.py:101
  137.3 23.4 %collective-permute-done.4 = bf16[64,16,512]{2,1,0:T(8,128)(2,1)} collective-permute-done((bf16[64,16,512]{2,1,0:T(8,128)(2,1)}, bf16[64,16,512]{2,1,0:T(8,128)(2,1)}, u32[]{:S(2)}, u32[]{:S(2)}) %collective-permute-start.4) | collective-permute-done | bytes 1048608 | tf_op jit(solution)/shard_map/ppermute | solution.py:101
  160.6 1.4 constant_dynamic-update-slice_fusion.7
  162.0 1.4 constant_dynamic-update-slice_fusion.6
  163.7 1.4 constant_dynamic-update-slice_fusion.3
  165.1 1.4 constant_dynamic-update-slice_fusion.2
  167.2 1.7 copy-done.3
  168.9 4.5 %fusion.3 = f32[1024,896]{1,0:T(8,128)S(1)} fusion(bf16[1024,2048]{1,0:T(8,128)(2,1)S(1)} %bitcast.55, bf16[1,2048,896]{2,1,0:T(8,128)(2,1)S(1)} %copy-done.3), kind=kOutput, calls=%fused_computation.7 | convolution fusion | flops 3758096384 | bytes 11534336 | tf_op jit(solution)/shard_map/dot_general | solution.py:106
  173.4 4.7 %multiply_convert_fusion = bf16[1024,896]{1,0:T(8,128)(2,1)S(1)} fusion(f32[1024,896]{1,0:T(8,128)S(1)} %fusion.3, bf16[1024,2048]{1,0:T(8,128)(2,1)S(1)} %bitcast.56, bf16[1,2048,896]{2,1,0:T(8,128)(2,1)S(1)} %copy-done.4), kind=kOutput, calls=%fused_computation.9 | convolution fusion | flops 3763601408 | bytes 13369344 | tf_op jit(solution)/shard_map/dot_general | solution.py:107
  178.1 6.1 %convolution_convert_fusion = bf16[1024,2048]{1,0:T(8,128)(2,1)} fusion(bf16[1024,896]{1,0:T(8,128)(2,1)S(1)} %multiply_convert_fusion, bf16[1,896,2048]{2,1,0:T(8,128)(2,1)S(1)} %copy-done.5), kind=kOutput, calls=%fused_computation.3 | convolution fusion | flops 3760193536 | bytes 9699328 | tf_op jit(solution)/shard_map/dot_general | solution.py:109
  184.2 48.8 %reduce-scatter.2.cloned.1.call-done = bf16[1024,512]{1,0:T(8,128)(2,1)} async-done(((bf16[1024,2048]{1,0:T(8,128)(2,1)}), bf16[1024,512]{1,0:T(8,128)(2,1)}) %reduce-scatter.2.cloned.1.call-update) | async-done | bytes 1048592 | tf_op jit(solution)/shard_map/reduce_scatter | solution.py:110
  232.9 10.7 %all-to-all-start.3 = ((bf16[64,16,512]{2,1,0:T(8,128)(2,1)}), bf16[64,16,512]{2,1,0:T(8,128)(2,1)S(1)}, u32[]{:S(2)}, u32[]{:S(2)}) async-start(bf16[64,16,512]{2,1,0:T(8,128)(2,1)} %bitcast.57), calls=%async_computation.4 | async-start | bytes 2097152 | tf_op jit(solution)/shard_map/all_to_all | solution.py:113
  243.8 28.0 %all-to-all-done.3 = bf16[64,16,512]{2,1,0:T(8,128)(2,1)S(1)} async-done(((bf16[64,16,512]{2,1,0:T(8,128)(2,1)}), bf16[64,16,512]{2,1,0:T(8,128)(2,1)S(1)}, u32[]{:S(2)}, u32[]{:S(2)}) %all-to-all-start.3) | async-done | bytes 1048608 | tf_op jit(solution)/shard_map/all_to_all | solution.py:113
  271.8 2.0 gather_fusion.1
  274.5 1.3 multiply_reduce_fusion
  (55 shorter events, 7.9 us)
Async XLA Ops:
  6.5 26.2 %copy-start = (bf16[512,512]{1,0:T(8,128)(2,1)S(1)}, bf16[512,512]{1,0:T(8,128)(2,1)}, u32[]{:S(2)}) copy-start(bf16[512,512]{1,0:T(8,128)(2,1)} %param.21) | copy-start | bytes 1572868
  6.5 35.6 %copy-start.1 = (f32[512]{0:T(512)S(1)}, f32[512]{0:T(512)}, u32[]{:S(2)}) copy-start(f32[512]{0:T(512)} %param.22) | copy-start | bytes 6148
  7.4 11.8 %collective-permute-start.1 = (bf16[2]{0:T(256)(128)(2,1)S(1)}, bf16[2]{0:T(256)(128)(2,1)S(1)}, u32[]{:S(2)}, u32[]{:S(2)}) collective-permute-start(bf16[2]{0:T(256)(128)(2,1)S(1)} %slice.41), channel_id=1, source_target_pairs={{0,4},{4,8},{8,12},{12,16},{16,20},{20,24},{24,28},{28,32},{32,36}... | collective-permute-start | bytes 20 | tf_op jit(solution)/shard_map/ppermute | solution.py:12
  12.8 7.3 %collective-permute-start = (bf16[2,128]{1,0:T(2,128)(2,1)S(1)}, bf16[2,128]{1,0:T(2,128)(2,1)S(1)}, u32[]{:S(2)}, u32[]{:S(2)}) collective-permute-start(bf16[2,128]{1,0:T(2,128)(2,1)S(1)} %slice.52), channel_id=1, source_target_pairs={{0,4},{4,8},{8,12},{12,16},{16,20},{20,24},{24,28},{28,32},{32,36}... | collective-permute-start | bytes 1544 | tf_op jit(solution)/shard_map/ppermute | solution.py:12
  21.9 9.9 %all-to-all-start = ((bf16[4,256,128]{1,2,0:T(8,128)(2,1)}), bf16[4,256,128]{1,2,0:T(8,128)(2,1)S(1)}, u32[]{:S(2)}, u32[]{:S(2)}) async-start(bf16[4,256,128]{1,2,0:T(8,128)(2,1)} %broadcast_in_dim.8), calls=%async_computation | async-start | bytes 524288 | tf_op jit(solution)/shard_map/all_to_all | solution.py:23
  34.7 7.4 %all-to-all-start.1 = ((f32[4,1,256]{2,1,0:T(1,128)}), f32[4,1,256]{2,1,0:T(1,128)S(1)}, u32[]{:S(2)}, u32[]{:S(2)}) async-start(f32[4,1,256]{2,1,0:T(1,128)} %broadcast_in_dim.9), calls=%async_computation.1 | async-start | bytes 8192 | tf_op jit(solution)/shard_map/all_to_all | solution.py:23
  37.9 195.0 %reduce-scatter.2.cloned.1.call-start = ((), (), s32[]{:S(2)}) async-start(), calls=%async_computation.5 | async-start | bytes 5242880 | tf_op jit(solution)/shard_map/reduce_scatter | solution.py:110
  88.4 24.8 %collective-permute-start.2 = (bf16[64,16,512]{2,1,0:T(8,128)(2,1)S(1)}, bf16[64,16,512]{2,1,0:T(8,128)(2,1)S(1)}, u32[]{:S(2)}, u32[]{:S(2)}) collective-permute-start(bf16[64,16,512]{2,1,0:T(8,128)(2,1)S(1)} %all_to_all.21), channel_id=1, source_target_pairs={{0,1},{1,2},{2,3},{3,0},{4,5},{5,6},{6,7},{7,4},{8,9},{9,10},{10,1... | collective-permute-start | bytes 3145736 | tf_op jit(solution)/shard_map/ppermute | solution.py:101
  113.2 24.0 %collective-permute-start.3 = (bf16[64,16,512]{2,1,0:T(8,128)(2,1)S(1)}, bf16[64,16,512]{2,1,0:T(8,128)(2,1)}, u32[]{:S(2)}, u32[]{:S(2)}) collective-permute-start(bf16[64,16,512]{2,1,0:T(8,128)(2,1)S(1)} %collective-permute-done.2), channel_id=1, source_target_pairs={{0,1},{1,2},{2,3},{3,0},{4,5},{5,6},{6,7},{7,4},{8,9},{9,10},{10,1... | collective-permute-start | bytes 3145736 | tf_op jit(solution)/shard_map/ppermute | solution.py:101
  137.2 23.4 %collective-permute-start.4 = (bf16[64,16,512]{2,1,0:T(8,128)(2,1)}, bf16[64,16,512]{2,1,0:T(8,128)(2,1)}, u32[]{:S(2)}, u32[]{:S(2)}) collective-permute-start(bf16[64,16,512]{2,1,0:T(8,128)(2,1)} %collective-permute-done.3), channel_id=1, source_target_pairs={{0,1},{1,2},{2,3},{3,0},{4,5},{5,6},{6,7},{7,4},{8,9},{9,10},{10,1... | collective-permute-start | bytes 3145736 | tf_op jit(solution)/shard_map/ppermute | solution.py:101
  166.8 2.0 copy-start.3
  168.9 4.5 %copy-start.4 = (bf16[1,2048,896]{2,1,0:T(8,128)(2,1)S(1)}, bf16[1,2048,896]{2,1,0:T(8,128)(2,1)}, u32[]{:S(2)}) copy-start(bf16[1,2048,896]{2,1,0:T(8,128)(2,1)} %param.26) | copy-start | bytes 11010052
  173.4 4.7 %copy-start.5 = (bf16[1,896,2048]{2,1,0:T(8,128)(2,1)S(1)}, bf16[1,896,2048]{2,1,0:T(8,128)(2,1)}, u32[]{:S(2)}) copy-start(bf16[1,896,2048]{2,1,0:T(8,128)(2,1)} %param.27) | copy-start | bytes 11010052
  184.1 59.5 %copy-start.2 = (f32[256,2]{0,1:T(2,128)S(1)}, f32[256,2]{0,1:T(2,128)}, u32[]{:S(2)}) copy-start(f32[256,2]{0,1:T(2,128)} %param.24) | copy-start | bytes 6148
  232.9 38.9 %all-to-all-start.3 = ((bf16[64,16,512]{2,1,0:T(8,128)(2,1)}), bf16[64,16,512]{2,1,0:T(8,128)(2,1)S(1)}, u32[]{:S(2)}, u32[]{:S(2)}) async-start(bf16[64,16,512]{2,1,0:T(8,128)(2,1)} %bitcast.57), calls=%async_computation.4 | async-start | bytes 2097152 | tf_op jit(solution)/shard_map/all_to_all | solution.py:113
Sparse Core Ops, SparseCore 0:
  184.3 48.5 reduce-scatter.1
